TPU v7x, 512 devices: a whole 4x4x16 slice. The times are simulated.
512 devices in a mesh: ep: 32 (over z, core), tp: 16 (over y, x).
Axes of the slice: x: 4, y: 4, z: 16, core: 2. Of those that a mesh axis runs over, the one named last changes fastest.
Arguments:
- query_vectors: bfloat16 [16384, 4096], P('ep', 'tp'), may hold values from -6 to 6
- key_vectors: bfloat16 [16384, 2048], P('ep', 'tp'), may hold values from -6 to 6
- value_vectors: bfloat16 [16384, 2048], P('ep', 'tp'), may hold values from -64 to 64
- query_gain: float32 [128], replicated, may hold values from 0.1 to 1.9
- key_gain: float32 [128], replicated, may hold values from 0.1 to 1.9
- sink_logits: float32 [32], P('tp'), may hold values from 3 to 7
- moe_rows: bfloat16 [5120, 4096], P('ep', 'tp'), may hold values from -6 to 6
- norm_gain: float32 [4096], replicated, may hold values from 0.1 to 1.9
- expert_ids: int32 [5120, 4], P('ep'), may hold values from 0 to 31, all different within a row; in each aligned block of 160 rows (0 to 159, 160 to 319, ...) at most 30 rows name the same one
- route_weights: float32 [5120, 4], P('ep'), may hold values from 0.25 to 2.5
- expert_gate: bfloat16 [32, 4096, 2048], P('ep', None, 'tp'), may hold values from -0.09375 to 0.09375
- expert_up: bfloat16 [32, 4096, 2048], P('ep', None, 'tp'), may hold values from -0.09375 to 0.09375
- expert_down: bfloat16 [32, 2048, 4096], P('ep', None, 'tp'), may hold values from -0.125 to 0.125
- shared_gate: bfloat16 [4096, 512], P(None, 'tp'), may hold values from -0.09375 to 0.09375
- shared_up: bfloat16 [4096, 512], P(None, 'tp'), may hold values from -0.09375 to 0.09375
- shared_down: bfloat16 [512, 4096], P(None, 'tp'), may hold values from -0.25 to 0.25
Outputs:
- attended: bfloat16 [16384, 4096], P('ep', 'tp')
- moe_out: bfloat16 [5120, 4096], P('ep', 'tp')
Inputs may be any that keep to these rules, and one draw needn't show every extreme that they name: `expert_ids`: each row names 4 different experts. Within the rows of one index of ep (aligned blocks of 160 rows), no expert is named by more than 30 rows, and in some block one expert is named by exactly 30.
All inputs are finite; a program needn't handle non-finite values.
Results may differ from a plain program's by a relative error of at most 0.0071.
Values may be sent and summed in bfloat16 or wider, within the bound.
A program may use at most 64 MiB of HBM per device.

v0:
```python
import numpy as np
import jax
import jax.numpy as jnp
from jax import lax
from jax.experimental import pallas as pl
from jax.experimental.pallas import tpu as pltpu
from jax.sharding import PartitionSpec as P

MESH = pl.DeviceIdType.MESH
BF = jnp.bfloat16
F32 = jnp.float32

HEAD_DIM = 128
WINDOW = 128
GRID_W = 64
D = 4096
TOP_K = 4
EPS = 1e-06
ROTARY_BASE = 10000.0

NZ = 16
TOK = 160
TPAD = 256
SLOT = 32
ROWS = 32 * SLOT
LEN = 512
FEAT = 256
UNITS = 128
PACK = 40

GROUPS = [[1, -1], [6, -6], [7, -7], [8], [5, -5], [4, -4], [3, -3], [2, -2], [0]]
REL = sum(GROUPS, [])
NCHUNK = len(GROUPS)
ZFIRST = [2 * SLOT * sum(len(g) for g in GROUPS[:c]) for c in range(NCHUNK)]
ZSIZE = [2 * SLOT * len(g) for g in GROUPS]
SIZE = [(60 * len(g) + 7) // 8 * 8 for g in GROUPS]
FIRST = [sum(SIZE[:c]) for c in range(NCHUNK)]
PACKED = sum(SIZE)
HERE = REL.index(0)
OWN_CHUNK = [c for c in range(NCHUNK) if 0 in GROUPS[c]][0]


def _inv(p):
    return REL.index(REL[p] if REL[p] in (0, 8) else -REL[p])


INV = [_inv(p) for p in range(NZ)]
CHUNK = 256

GATHER_1 = list(zip(FIRST, SIZE)) + [(PACKED, TOK)]
GATHER_2 = list(zip(FIRST, SIZE)) + [(PACKED, PACK)]
NGATHER = NCHUNK + 1

ORDER = (
    "R9", "zi:0", "halo", "zi:1", "zi:2", "zi:3", "zi:4", "zi:5", "zi:6", "zi:7", "zi:8",
    "cw", "lda", "lds", "ldb", "tq", "wi:8", "R8", "wi:0", "R0", "wh", "tk", "R9", "at:0",
    "at:1", "at:2", "at:3", "R8", "R0", "R9", "R8", "R0", "wi:1", "R1", "R9", "R8", "R0",
    "R1", "R9", "si", "H9", "wi:2", "R2", "R8", "ei:8", "H8", "R1", "R0", "ei:0", "H0",
    "wi:3", "R3", "R2", "H9", "H8", "wi:4", "R4", "R1", "H0", "R3", "R2", "wi:5", "R5",
    "H9", "H8", "R4", "R1", "ei:1", "H1", "H0", "R3", "R2", "R5", "H9", "H8", "R4", "H1",
    "H0", "R3", "R2", "ei:2", "H2", "R5", "H9", "so", "wi:6", "R6", "H1", "R4", "H8",
    "eo:8", "zo:8", "wi:7", "R7", "H0", "eo:0", "zo:0", "H2", "R3", "ei:3", "H3", "R5",
    "R6", "H1", "wo:0", "cb:0-128", "R4", "ei:4", "H4", "H2", "R7", "H3", "R5", "ei:5",
    "H5", "R6", "H1", "eo:1", "zo:1", "H2", "H4", "R7", "H3", "H5", "R6", "H2", "eo:2",
    "zo:2", "H4", "R7", "H3", "H5", "R6", "ei:6", "H6", "H4", "R7", "ei:7", "H7", "H5",
    "H3", "eo:3", "zo:3", "H6", "wo:1", "cb:128-256", "H4", "eo:4", "zo:4", "H7", "H5",
    "eo:5", "zo:5", "H6", "H7", "wo:2", "cb:256-384", "H6", "H7", "H6", "eo:6", "zo:6",
    "H7", "eo:7", "zo:7", "wo:3", "wo:4", "cb:384-512", "wo:5", "cb:512-640", "wo:6",
    "cb:640-768", "wo:7", "cb:768-896", "wo:8", "cb:896-1024", "end",
)


def up8(v):
    return (v + 7) // 8 * 8


def kernel(
    x_hbm,
    ids_hbm,
    rw_hbm,
    q_hbm,
    k_hbm,
    v_hbm,
    qg_hbm,
    kg_hbm,
    sink_hbm,
    ng_hbm,
    colt_hbm,
    rowt_hbm,
    gate_hbm,
    up_hbm,
    down_hbm,
    sg_hbm,
    su_hbm,
    sd_hbm,
    att_ref,
    out_ref,
    ids_ref,
    rw_ref,
    q_ref,
    qg_ref,
    kg_ref,
    sink_ref,
    ng_ref,
    colt_ref,
    sg_ref,
    su_ref,
    xg,
    hg,
    wgu,
    wd,
    wsd,
    rowt,
    kpad,
    vpad,
    qt,
    kt,
    xpad,
    idsp,
    rwp,
    send,
    wt_hi,
    wt_lo,
    lhs,
    res,
    ret,
    acc,
    sh_acc,
    zst,
    pick,
    spread,
    g_send,
    g_recv,
    zi_send,
    zi_recv,
    zo_send,
    zo_recv,
    halo_sem,
    loc,
):
    ep = lax.axis_index("ep")
    tp = lax.axis_index("tp")
    z = ep // 2
    core = ep % 2
    y = tp // 4
    x = tp % 4
    xr, xl = (x + 1) % 4, (x + 3) % 4
    yr, yl = (y + 1) % 4, (y + 3) % 4
    xo, yo = (x + 2) % 4, (y + 2) % 4

    def ep_at(rel, c):
        return ((z + rel + NZ) % NZ) * 2 + c

    ep_hi = (ep + 1) % 32
    ep_lo = (ep + 31) % 32

    barrier = pltpu.get_barrier_semaphore()
    for p in range(NZ):
        for c in range(2):
            if REL[p] == 0:
                continue
            pl.semaphore_signal(
                barrier, inc=1, device_id={"ep": ep_at(REL[p], c), "tp": tp}, device_id_type=MESH
            )
    pl.semaphore_signal(
        barrier, inc=1, device_id={"ep": z * 2 + (1 - core), "tp": tp}, device_id_type=MESH
    )
    plane = [y * 4 + xr, y * 4 + xl, yr * 4 + x, yl * 4 + x]
    for t in plane:
        pl.semaphore_signal(barrier, inc=1, device_id={"ep": ep, "tp": t}, device_id_type=MESH)

    def load(i, src, dst):
        cp = pltpu.make_async_copy(src, dst, loc.at[i])
        cp.start()
        return cp

    mid = pl.ds(WINDOW, LEN)
    rows_at = pl.ds(PACKED, TOK)
    ld_own = load(0, x_hbm, xg.at[y, x, rows_at])
    ld_route = [
        load(1, ids_hbm, ids_ref),
        load(2, rw_hbm, rw_ref),
        load(3, x_hbm, xpad.at[pl.ds(0, TOK)]),
    ]
    ld_kv = [load(4, k_hbm, kpad.at[mid]), load(5, v_hbm, vpad.at[mid])]
    ld_att = [
        load(6, q_hbm, q_ref),
        load(7, qg_hbm, qg_ref),
        load(8, kg_hbm, kg_ref),
        load(9, sink_hbm, sink_ref),
        load(10, colt_hbm, colt_ref),
        load(11, rowt_hbm.at[:, pl.ds(pl.multiple_of(ep * 8, 8), 16), :], rowt),
    ]
    ld_shared = [load(12, sg_hbm, sg_ref), load(13, su_hbm, su_ref), load(14, ng_hbm, ng_ref)] + [
        load(15 + j, sd_hbm, wsd.at[:, pl.ds(32 * j, 32), :]) for j in range(4)
    ]
    ld_big = [
        load(19, gate_hbm.at[0], wgu.at[:, 0:128]),
        load(20, up_hbm.at[0], wgu.at[:, 128:256]),
        load(21, down_hbm.at[0], wd),
    ]

    def wait_all(copies):
        for cp in copies:
            cp.wait()

    xpad[TOK:TPAD, :] = jnp.zeros((TPAD - TOK, FEAT), BF)
    idsp[...] = jnp.full(idsp.shape, -1, jnp.int32)
    rwp[...] = jnp.zeros_like(rwp)
    wait_all(ld_route)
    idsp[0:TOP_K, 0:TOK] = ids_ref[...]
    rwp[0:TOP_K, 0:TOK] = rw_ref[...]

    row32 = lax.broadcasted_iota(jnp.int32, (32, TPAD), 0)
    pos32 = row32 >> 1
    rel32 = jnp.zeros((32, TPAD), jnp.int32)
    for p in range(NZ):
        rel32 = jnp.where(pos32 == p, REL[p] + NZ, rel32)
    expert32 = ((z + rel32) & (NZ - 1)) * 2 + (row32 & 1)
    named = jnp.zeros((32, TPAD), F32)
    weight = jnp.zeros((32, TPAD), F32)
    for k in range(TOP_K):
        same = idsp[k : k + 1, :] == expert32
        named = jnp.where(same, 1.0, named)
        weight = jnp.where(same, rwp[k : k + 1, :], weight)
    before = (
        lax.broadcasted_iota(jnp.int32, (TPAD, TPAD), 0)
        < lax.broadcasted_iota(jnp.int32, (TPAD, TPAD), 1)
    )
    count = jnp.dot(
        named.astype(BF), jnp.where(before, 1.0, 0.0).astype(BF), preferred_element_type=F32
    )
    slot32 = jnp.where(named > 0.5, count, -1.0)
    slot_row = lax.broadcasted_iota(jnp.int32, (SLOT, TPAD), 0).astype(F32)
    for t in range(NCHUNK):
        lo, n = ZFIRST[t], ZSIZE[t]
        picks = [
            jnp.where(slot32[i : i + 1, :] == slot_row, 1.0, 0.0).astype(BF)
            for i in range(lo // SLOT, (lo + n) // SLOT)
        ]
        send[lo : lo + n, :] = jnp.dot(
            jnp.concatenate(picks, axis=0), xpad[...], preferred_element_type=F32
        ).astype(BF)
    mine = pl.ds(pl.multiple_of(HERE * 2 * SLOT + core * SLOT, SLOT), SLOT)
    other = pl.ds(pl.multiple_of(HERE * 2 * SLOT + (1 - core) * SLOT, SLOT), SLOT)
    zst[mine, :] = send[mine, :]

    def moved(r):
        over = [jnp.where(r >= 30 * i, 2, 0) for i in (1, 2, 3)]
        return r + over[0] + over[1] + over[2]

    iota = lambda shape, axis: lax.broadcasted_iota(jnp.int32, shape, axis)
    wide_shape, tall_shape = (120, 128), (128, 120)
    pick[...] = jnp.where(
        moved(iota(wide_shape, 0)) == iota(wide_shape, 1), 1.0, 0.0
    ).astype(BF)
    spread[...] = jnp.where(
        iota(tall_shape, 0) == moved(iota(tall_shape, 1)), 1.0, 0.0
    ).astype(BF)

    def pack(c):
        rows = jnp.dot(
            pick[0 : SIZE[c], 0 : ZSIZE[c]],
            zst[ZFIRST[c] : ZFIRST[c] + ZSIZE[c], :],
            preferred_element_type=F32,
        )
        xg[y, x, FIRST[c] : FIRST[c] + SIZE[c], :] = rows.astype(BF)

    ld_own.wait()
    pl.semaphore_wait(barrier, 35)

    ends = []

    def remote(src, dst, ssem, rsem, dev):
        cp = pltpu.make_async_remote_copy(
            src_ref=src,
            dst_ref=dst,
            send_sem=ssem,
            recv_sem=rsem,
            device_id=dev,
            device_id_type=MESH,
        )
        return cp

    partner = {"ep": z * 2 + (1 - core), "tp": tp}

    class Gather:
        def __init__(self, which, buf, start, size, index):
            self.buf, self.width = buf, buf.shape[3]
            self.start, self.size = start, size
            self.index = which * NGATHER + index
            na = up8(size // 2)
            self.ranges = []
            for first, count in ((start, na), (start + na, size - na)):
                self.ranges.append((first, count, up8(count // 2)))
            self.stage = 0

        def next(self):
            s = self.stage
            self.stage += 1
            buf = self.buf
            ssem = g_send.at[self.index]
            if s > 0:
                rows = pl.ds(self.start, self.size)
                whole = (
                    buf.at[pl.ds(0, 2), 0, rows],
                    buf.at[0, 0, rows],
                    buf.at[pl.ds(0, 2), :, rows],
                    buf.at[0, :, rows],
                )[s - 1]
                rsem = g_recv.at[self.index * 4 + s - 1]
                remote(whole, whole, ssem, rsem, partner).wait_recv()
            if s == 4:
                whole = lhs.at[pl.ds(0, 15), pl.ds(0, self.size), pl.ds(0, self.width)]
                ends.append(remote(whole, whole, ssem, g_recv.at[self.index * 4], partner))
                return
            near, wide = [], []
            for half, (first, count, low) in enumerate(self.ranges):
                full = pl.ds(first, count)
                part_lo, part_hi = pl.ds(first, low), pl.ds(first + low, count - low)
                if half == 0:
                    piece = lambda w, v, r: buf.at[w, v, r]
                    group = lambda w, r: buf.at[w, :, r]
                    n_me, n_r, n_l, n_o, w_me, w_r, w_l = x, xr, xl, xo, y, yr, yl
                    to_n, to_w = (y * 4 + xr, y * 4 + xl), (yr * 4 + x, yl * 4 + x)
                else:
                    piece = lambda w, v, r: buf.at[v, w, r]
                    group = lambda w, r: buf.at[:, w, r]
                    n_me, n_r, n_l, n_o, w_me, w_r, w_l = y, yr, yl, yo, x, xr, xl
                    to_n, to_w = (yr * 4 + x, yl * 4 + x), (y * 4 + xr, y * 4 + xl)
                if s == 0:
                    near += [(piece(w_me, n_me, full), to, 0) for to in to_n]
                    wide += [(piece(w_me, n_me, full), to, 2) for to in to_w]
                elif s == 1:
                    near += [
                        (piece(w_me, n_l, part_lo), to_n[0], 1),
                        (piece(w_me, n_r, part_hi), to_n[1], 1),
                    ]
                    wide += [(piece(w_me, v, full), to, 2) for v in (n_l, n_r) for to in to_w]
                elif s == 2:
                    wide += [(piece(w_me, n_o, full), to, 2) for to in to_w]
                else:
                    wide += [
                        (group(w_l, part_lo), to_w[0], 3),
                        (group(w_r, part_hi), to_w[1], 3),
                    ]
            for ref, to, kind in near + wide:
                remote(
                    ref, ref, ssem, g_recv.at[self.index * 4 + kind], {"ep": ep, "tp": to}
                ).start()

    rows_g = [Gather(0, xg, s, n, i) for i, (s, n) in enumerate(GATHER_1)]
    hid_g = [Gather(1, hg, s, n, i) for i, (s, n) in enumerate(GATHER_2)]

    def z_start(chunk, src_at, dst_at, ssem, rsem):
        for p in range(ZFIRST[chunk] // (2 * SLOT), (ZFIRST[chunk] + ZSIZE[chunk]) // (2 * SLOT)):
            q = INV[p]
            back = pl.ds(pl.multiple_of(q * 2 * SLOT + core * SLOT, SLOT), SLOT)
            if REL[p] == 0:
                pieces = [(other, partner)]
            else:
                pieces = [
                    (
                        pl.ds(p * 2 * SLOT + c * SLOT, SLOT),
                        {"ep": ep_at(REL[p], c), "tp": tp},
                    )
                    for c in range(2)
                ]
            for rows, dev in pieces:
                remote(src_at(rows), dst_at(back), ssem.at[chunk], rsem.at[chunk], dev).start()
        rows = other if chunk == OWN_CHUNK else pl.ds(ZFIRST[chunk], ZSIZE[chunk])
        ends.append(remote(src_at(rows), src_at(rows), ssem.at[chunk], rsem.at[chunk], partner))

    def z_wait(chunk, at, rsem, ssem):
        rows = other if chunk == OWN_CHUNK else pl.ds(ZFIRST[chunk], ZSIZE[chunk])
        remote(at(rows), at(rows), ssem.at[chunk], rsem.at[chunk], partner).wait_recv()

    own_at = lambda r: zst.at[r]
    send_at = lambda r: send.at[r]
    res_at = lambda r: res.at[r]
    ret_at = lambda r: ret.at[r]

    def start_zin(chunk):
        z_start(chunk, send_at, own_at, zi_send, zi_recv)

    def wait_zin(chunk):
        z_wait(chunk, own_at, zi_recv, zi_send)
        pack(chunk)

    def start_zout(chunk):
        z_start(chunk, res_at, ret_at, zo_send, zo_recv)

    def wait_zout(chunk):
        z_wait(chunk, ret_at, zo_recv, zo_send)

    def start_halo():
        tail, head = pl.ds(LEN, WINDOW), pl.ds(WINDOW, WINDOW)
        wait_all(ld_kv)
        for i, pad in enumerate((kpad, vpad)):
            for j, (part, to, at) in enumerate(
                ((tail, ep_hi, pl.ds(0, WINDOW)), (head, ep_lo, pl.ds(WINDOW + LEN, WINDOW)))
            ):
                cp = remote(
                    pad.at[part],
                    pad.at[at],
                    halo_sem.at[0],
                    halo_sem.at[1],
                    {"ep": to, "tp": tp},
                )
                cp.start()
        ends.append(halo_all())

    def halo_all():
        ref = kpad.at[pl.ds(0, 4 * WINDOW)]
        return remote(ref, ref, halo_sem.at[0], halo_sem.at[1], partner)

    first_half = (lax.broadcasted_iota(jnp.int32, (GRID_W, HEAD_DIM), 1) & 63) < 32

    def turn(raw, gain, g):
        f = raw.astype(F32)
        n = f * lax.rsqrt(jnp.mean(f * f, axis=-1, keepdims=True) + EPS) * gain
        other = jnp.where(first_half, pltpu.roll(n, 96, 1), pltpu.roll(n, 32, 1))
        cos = rowt[0, pl.ds(g, 1), :] + colt_ref[0]
        sin = rowt[1, pl.ds(g, 1), :] + colt_ref[1]
        return (n * cos + other * sin).astype(BF)

    def turn_queries():
        for g in range(LEN // GRID_W):
            for h in range(2):
                rows = slice(g * GRID_W, (g + 1) * GRID_W)
                qt[h, rows, :] = turn(
                    q_ref[rows, h * HEAD_DIM : (h + 1) * HEAD_DIM], qg_ref[...], g + 2
                )

    def turn_keys():
        for g in range((LEN + 2 * WINDOW) // GRID_W):
            rows = slice(g * GRID_W, (g + 1) * GRID_W)
            kt[rows, :] = turn(kpad[rows, :], kg_ref[...], g)

    near_q = lax.broadcasted_iota(jnp.int32, (128, 384), 0)
    near_k = lax.broadcasted_iota(jnp.int32, (128, 384), 1)

    def attend(b):
        key_pos = near_k + (ep * LEN - WINDOW + 128 * b)
        inside = (
            (near_k >= near_q)
            & (near_k <= near_q + 2 * WINDOW)
            & (key_pos >= 0)
            & (key_pos < 32 * LEN)
        )
        keys = kt[128 * b : 128 * b + 384, :]
        values = vpad[128 * b : 128 * b + 384, :]
        for h in range(2):
            scores = lax.dot_general(
                qt[h, 128 * b : 128 * b + 128, :],
                keys,
                (((1,), (1,)), ((), ())),
                preferred_element_type=F32,
            ) * (HEAD_DIM ** (-0.5))
            raised = jnp.where(inside, jnp.exp(scores), 0.0)
            sink = jnp.exp(jnp.full((128, 1), sink_ref[h], F32))
            den = sink + jnp.sum(raised, axis=-1, keepdims=True)
            weights = (raised * (1.0 / den)).astype(BF)
            mixed = jnp.dot(weights, values, preferred_element_type=F32)
            att_ref[128 * b : 128 * b + 128, h * 128 : (h + 1) * 128] = mixed.astype(BF)

    def scale_rows(start, size):
        acc[0:size, 0:128] = jnp.zeros((size, 128), F32)

        def one(s, carry):
            f = xg[s // 4, s % 4, start : start + size, :].astype(F32)
            sq = f * f
            acc[0:size, 0:128] += sq[:, 0:128] + sq[:, 128:256]
            lhs[s, 0:size, :] = (f * ng_ref[:, pl.ds(pl.multiple_of(s * FEAT, FEAT), FEAT)]).astype(BF)
            return carry

        lax.fori_loop(0, 16, one, 0)
        return lax.rsqrt(jnp.sum(acc[0:size, 0:128], axis=-1, keepdims=True) / D + EPS)

    def activate(g, u, factor):
        g, u = g * factor, u * factor
        return (g / (1.0 + jnp.exp(-g)) * u).astype(BF)

    def experts_in(c):
        start, size = FIRST[c], SIZE[c]
        factor = scale_rows(start, size)
        both = jnp.dot(
            jnp.concatenate([lhs[s, 0:size, :] for s in range(16)], axis=1),
            wgu[...],
            preferred_element_type=F32,
        )
        hg[y, x, start : start + size, :] = activate(both[:, 0:128], both[:, 128:256], factor)

    def shared_in():
        factor = scale_rows(PACKED, TOK)
        rows = jnp.concatenate([lhs[s, 0:TOK, :] for s in range(16)], axis=1)
        across = (((1,), (1,)), ((), ()))
        g = lax.dot_general(rows, sg_ref[...], across, preferred_element_type=F32)
        u = lax.dot_general(rows, su_ref[...], across, preferred_element_type=F32)
        h = activate(g, u, factor).astype(F32)
        packed = jnp.concatenate([h[40 * j : 40 * j + 40, :] for j in range(4)], axis=1)
        hg[y, x, PACKED : PACKED + PACK, :] = packed.astype(BF)

    def experts_out(c):
        start, size = FIRST[c], SIZE[c]
        rows = jnp.concatenate(
            [hg[s // 4, s % 4, start : start + size, :] for s in range(16)], axis=1
        )
        packed = jnp.dot(rows, wd[...], preferred_element_type=F32).astype(BF)
        res[ZFIRST[c] : ZFIRST[c] + ZSIZE[c], :] = jnp.dot(
            spread[0 : ZSIZE[c], 0:size], packed, preferred_element_type=F32
        ).astype(BF)
        if c == OWN_CHUNK:
            ret[mine, :] = res[mine, :]

    def shared_out():
        group = lax.broadcasted_iota(jnp.int32, (40, 128), 1) // 32
        total = jnp.zeros((TOK, FEAT), F32)
        for s in range(16):
            piece = hg[s // 4, s % 4, PACKED : PACKED + PACK, :].astype(F32)[0:40, :]
            parts = jnp.concatenate(
                [jnp.where(group == j, piece, 0.0) for j in range(4)], axis=0
            )
            total += jnp.dot(parts.astype(BF), wsd[s], preferred_element_type=F32)
        sh_acc[...] = total

    def combine_weights():
        for t in range(ROWS // CHUNK):
            full = jnp.concatenate(
                [
                    jnp.where(slot32[i : i + 1, :] == slot_row, weight[i : i + 1, :], 0.0)
                    for i in range(8 * t, 8 * t + 8)
                ],
                axis=0,
            )
            turned = jnp.transpose(full)
            high = turned.astype(BF)
            rows = slice(t * CHUNK, (t + 1) * CHUNK)
            wt_hi[:, rows] = high
            wt_lo[:, rows] = (turned - high.astype(F32)).astype(BF)

    def combine(lo, hi):
        rows = ret[lo:hi, :]
        part = jnp.dot(wt_hi[:, lo:hi], rows, preferred_element_type=F32) + jnp.dot(
            wt_lo[:, lo:hi], rows, preferred_element_type=F32
        )
        sh_acc[...] += part[0:TOK, :]

    gathers = {f"R{c}": g for c, g in enumerate(rows_g)} | {f"H{c}": g for c, g in enumerate(hid_g)}

    def wait_halo():
        halo_all().wait_recv()

    def finish():
        out_ref[...] = sh_acc[...].astype(BF)
        for cp in ends:
            cp.wait_send()

    calls = dict(
        zi=start_zin,
        halo=start_halo,
        cw=combine_weights,
        tq=turn_queries,
        tk=turn_keys,
        wh=wait_halo,
        wi=wait_zin,
        zo=start_zout,
        wo=wait_zout,
        at=attend,
        si=shared_in,
        so=shared_out,
        ei=experts_in,
        eo=experts_out,
        cb=combine,
        lda=lambda: wait_all(ld_att),
        lds=lambda: wait_all(ld_shared),
        ldb=lambda: wait_all(ld_big),
        end=finish,
    )
    for item in ORDER:
        with jax.named_scope(item):
            if item in gathers:
                gathers[item].next()
            else:
                name, _, arg = item.partition(":")
                calls[name](*[int(v) for v in arg.split("-") if v])


def deliver(a_in, b_in, a_out, b_out, sems):
    copies = [
        pltpu.make_async_copy(a_in, a_out, sems.at[0]),
        pltpu.make_async_copy(b_in, b_out, sems.at[1]),
    ]
    for cp in copies:
        cp.start()
    for cp in copies:
        cp.wait()


def _tables():
    quarter = HEAD_DIM // 4
    freq = np.float32(ROTARY_BASE) ** (
        np.float32(-4.0) * np.arange(quarter, dtype=np.float32) / np.float32(HEAD_DIM)
    )
    freq = freq.astype(np.float32)
    sign = np.concatenate([-np.ones(quarter), np.ones(quarter)])

    def of(index):
        angle = (index.astype(np.float32)[:, None] * freq).astype(np.float32).astype(np.float64)
        angle = np.concatenate([angle, angle], axis=1)
        return np.cos(angle), np.sin(angle) * sign

    def put(pair, left):
        pads = [(0, 0), (0, 64)] if left else [(0, 0), (64, 0)]
        return np.stack([np.pad(v, pads) for v in pair]).astype(np.float32)

    rows = put(of(np.arange(-2, 270)), True)
    cols = put(of(np.arange(GRID_W)), False)
    return rows, cols


ROW_TABLE, COL_TABLE = _tables()


def shards(
    query_vectors,
    key_vectors,
    value_vectors,
    query_gain,
    key_gain,
    sink_logits,
    moe_rows,
    norm_gain,
    expert_ids,
    route_weights,
    expert_gate,
    expert_up,
    expert_down,
    shared_gate,
    shared_up,
    shared_down,
):
    vm = pl.BlockSpec(memory_space=pltpu.VMEM)
    hb = pl.BlockSpec(memory_space=pl.ANY)
    dma = pltpu.SemaphoreType.DMA
    made = pl.pallas_call(
        kernel,
        out_shape=(
            jax.ShapeDtypeStruct((LEN, 2 * HEAD_DIM), BF),
            jax.ShapeDtypeStruct((TOK, FEAT), BF),
        ),
        in_specs=[hb] * 18,
        out_specs=(vm, vm),
        scratch_shapes=[
            pltpu.VMEM((TOP_K, TOK), jnp.int32),
            pltpu.VMEM((TOP_K, TOK), F32),
            pltpu.VMEM((LEN, 2 * HEAD_DIM), BF),
            pltpu.VMEM((1, HEAD_DIM), F32),
            pltpu.VMEM((1, HEAD_DIM), F32),
            pltpu.SMEM((2,), F32),
            pltpu.VMEM((1, D), F32),
            pltpu.VMEM((2, GRID_W, HEAD_DIM), F32),
            pltpu.VMEM((32, D), BF),
            pltpu.VMEM((32, D), BF),
            pltpu.VMEM((4, 4, PACKED + TOK, FEAT), BF),
            pltpu.VMEM((4, 4, PACKED + PACK, UNITS), BF),
            pltpu.VMEM((D, 2 * UNITS), BF),
            pltpu.VMEM((16 * UNITS, FEAT), BF),
            pltpu.VMEM((16, 128, FEAT), BF),
            pltpu.VMEM((2, 16, 128), F32),
            pltpu.VMEM((LEN + 2 * WINDOW, HEAD_DIM), BF),
            pltpu.VMEM((LEN + 2 * WINDOW, HEAD_DIM), BF),
            pltpu.VMEM((2, LEN, HEAD_DIM), BF),
            pltpu.VMEM((LEN + 2 * WINDOW, HEAD_DIM), BF),
            pltpu.VMEM((TPAD, FEAT), BF),
            pltpu.VMEM((8, TPAD), jnp.int32),
            pltpu.VMEM((8, TPAD), F32),
            pltpu.VMEM((ROWS, FEAT), BF),
            pltpu.VMEM((TPAD, ROWS), BF),
            pltpu.VMEM((TPAD, ROWS), BF),
            pltpu.VMEM((16, CHUNK, FEAT), BF),
            pltpu.VMEM((ROWS, FEAT), BF),
            pltpu.VMEM((ROWS, FEAT), BF),
            pltpu.VMEM((CHUNK, 128), F32),
            pltpu.VMEM((TOK, FEAT), F32),
            pltpu.VMEM((ROWS, FEAT), BF),
            pltpu.VMEM((120, 128), BF),
            pltpu.VMEM((128, 120), BF),
            dma((2 * NGATHER,)),
            dma((8 * NGATHER,)),
            dma((NCHUNK,)),
            dma((NCHUNK,)),
            dma((NCHUNK,)),
            dma((NCHUNK,)),
            dma((2,)),
            dma((22,)),
        ],
        compiler_params=pltpu.CompilerParams(
            collective_id=0, has_side_effects=True, vmem_limit_bytes=67043328
        ),
        name="fused",
    )(
        moe_rows,
        expert_ids.T,
        route_weights.T,
        query_vectors,
        key_vectors,
        value_vectors,
        query_gain.reshape(1, HEAD_DIM),
        key_gain.reshape(1, HEAD_DIM),
        sink_logits,
        norm_gain.reshape(1, D),
        jnp.asarray(COL_TABLE),
        jnp.asarray(ROW_TABLE),
        expert_gate,
        expert_up,
        expert_down,
        shared_gate.T,
        shared_up.T,
        shared_down.reshape(16, 32, FEAT),
    )
    return pl.pallas_call(
        deliver,
        out_shape=tuple(jax.ShapeDtypeStruct(v.shape, v.dtype) for v in made),
        in_specs=[vm, vm],
        out_specs=(hb, hb),
        scratch_shapes=[dma((2,))],
        name="deliver",
    )(*made)


def solution(mesh):
    placed = (
        P("ep", "tp"),
        P("ep", "tp"),
        P("ep", "tp"),
        P(),
        P(),
        P("tp"),
        P("ep", "tp"),
        P(),
        P("ep", None),
        P("ep", None),
        P("ep", None, "tp"),
        P("ep", None, "tp"),
        P("ep", None, "tp"),
        P(None, "tp"),
        P(None, "tp"),
        P(None, "tp"),
    )
    return jax.shard_map(
        shards,
        mesh=mesh,
        in_specs=placed,
        out_specs=(P("ep", "tp"), P("ep", "tp")),
        check_vma=False,
    )
```

profile of v0, /device:TPU:1, one launch (start us, length us, event | category | flops | bytes accessed | tf_op | source)
XLA Modules:
  0.0 115.1 jit_solution(9336006428145375136)
XLA Ops:
  0.6 112.6 %fused.1 = (bf16[512,256]{1,0:T(8,128)(2,1)}, bf16[160,256]{1,0:T(8,128)(2,1)}) custom-call(bf16[160,256]{1,0:T(8,128)(2,1)} %x_hbm.1, s32[4,160]{1,0:T(4,128)} %bitcast.12, f32[4,160]{1,0:T(4,128)} %bitcast.13, bf16[512,256]{1,0:T(8,128)(2,1)} %q_hbm.1, bf16[512,128]{1,0:T(8,128)(2,1)} %k_hbm.1, bf16[512,128]{1,0:T(8,128)(2,1)} %v_hbm.1, ...), custom_call_target="tpu_custom_call" | custom-call | tf_op jit(solution)/shard_map/fused/pallas_call | solution.py:646
  113.2 1.7 %deliver.1 = (bf16[512,256]{1,0:T(8,128)(2,1)}, bf16[160,256]{1,0:T(8,128)(2,1)}) custom-call(bf16[512,256]{1,0:T(8,128)(2,1)} %get-tuple-element.4.a_in, bf16[160,256]{1,0:T(8,128)(2,1)} %get-tuple-element.5.b_in), custom_call_target="tpu_custom_call" | custom-call | tf_op jit(solution)/shard_map/deliver/pallas_call | solution.py:722
where the time goes:
time: 115 us
  Pallas kernels  114 us (99%)
    pallas_call x1, Pallas kernels, shards(): pl.pallas_call(kernel, out_shape=(jax.ShapeDtypeStruct((LEN, 2 * HEAD_DIM...  113 us

commit v1 on v0

--- a/solution.py
+++ b/solution.py
@@ -28,7 +28,7 @@
 UNITS = 128
 PACK = 40
 
-GROUPS = [[1, -1], [6, -6], [7, -7], [8], [5, -5], [4, -4], [3, -3], [2, -2], [0]]
+GROUPS = [[1, -1], [5, -5], [6, -6], [8], [7, -7], [4, -4], [0], [3, -3], [2, -2]]
 REL = sum(GROUPS, [])
 NCHUNK = len(GROUPS)
 ZFIRST = [2 * SLOT * sum(len(g) for g in GROUPS[:c]) for c in range(NCHUNK)]
@@ -53,20 +53,20 @@
 
 ORDER = (
     "R9", "zi:0", "halo", "zi:1", "zi:2", "zi:3", "zi:4", "zi:5", "zi:6", "zi:7", "zi:8",
-    "cw", "lda", "lds", "ldb", "tq", "wi:8", "R8", "wi:0", "R0", "wh", "tk", "R9", "at:0",
-    "at:1", "at:2", "at:3", "R8", "R0", "R9", "R8", "R0", "wi:1", "R1", "R9", "R8", "R0",
-    "R1", "R9", "si", "H9", "wi:2", "R2", "R8", "ei:8", "H8", "R1", "R0", "ei:0", "H0",
-    "wi:3", "R3", "R2", "H9", "H8", "wi:4", "R4", "R1", "H0", "R3", "R2", "wi:5", "R5",
-    "H9", "H8", "R4", "R1", "ei:1", "H1", "H0", "R3", "R2", "R5", "H9", "H8", "R4", "H1",
-    "H0", "R3", "R2", "ei:2", "H2", "R5", "H9", "so", "wi:6", "R6", "H1", "R4", "H8",
-    "eo:8", "zo:8", "wi:7", "R7", "H0", "eo:0", "zo:0", "H2", "R3", "ei:3", "H3", "R5",
-    "R6", "H1", "wo:0", "cb:0-128", "R4", "ei:4", "H4", "H2", "R7", "H3", "R5", "ei:5",
-    "H5", "R6", "H1", "eo:1", "zo:1", "H2", "H4", "R7", "H3", "H5", "R6", "H2", "eo:2",
-    "zo:2", "H4", "R7", "H3", "H5", "R6", "ei:6", "H6", "H4", "R7", "ei:7", "H7", "H5",
-    "H3", "eo:3", "zo:3", "H6", "wo:1", "cb:128-256", "H4", "eo:4", "zo:4", "H7", "H5",
-    "eo:5", "zo:5", "H6", "H7", "wo:2", "cb:256-384", "H6", "H7", "H6", "eo:6", "zo:6",
-    "H7", "eo:7", "zo:7", "wo:3", "wo:4", "cb:384-512", "wo:5", "cb:512-640", "wo:6",
-    "cb:640-768", "wo:7", "cb:768-896", "wo:8", "cb:896-1024", "end",
+    "cw", "lda", "lds", "ldb", "wi:6", "R6", "wi:0", "R0", "tq", "R9", "R6", "wh", "tk",
+    "R0", "at:0", "R9", "wi:1", "R1", "R0", "R6", "at:1", "R9", "R1", "R0", "wi:2", "R2",
+    "R9", "si", "H9", "R1", "R6", "wi:3", "R3", "R2", "R0", "ei:0", "H0", "R1", "R3", "R2",
+    "wi:4", "R4", "H9", "H0", "R6", "ei:6", "H6", "R1", "ei:1", "H1", "R2", "R3", "R4",
+    "wi:5", "R5", "H9", "H0", "H1", "wi:7", "R7", "R2", "ei:2", "H2", "R3", "R4", "R5",
+    "H9", "H0", "H1", "R7", "H2", "R3", "ei:3", "H3", "R4", "R5", "wi:8", "R8", "H9", "so",
+    "H1", "H0", "eo:0", "zo:0", "R7", "H2", "H3", "at:2", "R4", "ei:4", "H4", "R5", "H1",
+    "eo:1", "zo:1", "H3", "R7", "H2", "R8", "H4", "at:3", "R5", "ei:5", "H5", "H3", "R7",
+    "ei:7", "H7", "H2", "eo:2", "zo:2", "R8", "H4", "H5", "H3", "eo:3", "zo:3", "R8", "H4",
+    "H5", "H6", "H7", "wo:0", "cb:0-128", "wo:1", "cb:128-256", "R8", "ei:8", "H8", "H4",
+    "eo:4", "zo:4", "H5", "H6", "H7", "wo:2", "cb:256-384", "H8", "H5", "eo:5", "zo:5",
+    "H6", "H8", "H7", "H6", "eo:6", "zo:6", "H8", "H7", "eo:7", "zo:7", "H8", "eo:8",
+    "zo:8", "wo:3", "wo:4", "cb:384-512", "wo:5", "cb:512-640", "wo:6", "cb:640-768",
+    "wo:7", "cb:768-896", "wo:8", "cb:896-1024", "end",
 )
 
 
@@ -308,11 +308,11 @@
                     buf.at[pl.ds(0, 2), :, rows],
                     buf.at[0, :, rows],
                 )[s - 1]
-                rsem = g_recv.at[self.index * 4 + s - 1]
+                rsem = g_recv.at[self.index * 3 + (s - 1) % 3]
                 remote(whole, whole, ssem, rsem, partner).wait_recv()
             if s == 4:
                 whole = lhs.at[pl.ds(0, 15), pl.ds(0, self.size), pl.ds(0, self.width)]
-                ends.append(remote(whole, whole, ssem, g_recv.at[self.index * 4], partner))
+                ends.append(remote(whole, whole, ssem, g_recv.at[self.index * 3], partner))
                 return
             near, wide = [], []
             for half, (first, count, low) in enumerate(self.ranges):
@@ -346,7 +346,7 @@
                     ]
             for ref, to, kind in near + wide:
                 remote(
-                    ref, ref, ssem, g_recv.at[self.index * 4 + kind], {"ep": ep, "tp": to}
+                    ref, ref, ssem, g_recv.at[self.index * 3 + kind % 3], {"ep": ep, "tp": to}
                 ).start()
 
     rows_g = [Gather(0, xg, s, n, i) for i, (s, n) in enumerate(GATHER_1)]
@@ -367,13 +367,11 @@
                     for c in range(2)
                 ]
             for rows, dev in pieces:
-                remote(src_at(rows), dst_at(back), ssem.at[chunk], rsem.at[chunk], dev).start()
-        rows = other if chunk == OWN_CHUNK else pl.ds(ZFIRST[chunk], ZSIZE[chunk])
-        ends.append(remote(src_at(rows), src_at(rows), ssem.at[chunk], rsem.at[chunk], partner))
+                remote(src_at(rows), dst_at(back), ssem.at[0], rsem.at[chunk], dev).start()
 
     def z_wait(chunk, at, rsem, ssem):
         rows = other if chunk == OWN_CHUNK else pl.ds(ZFIRST[chunk], ZSIZE[chunk])
-        remote(at(rows), at(rows), ssem.at[chunk], rsem.at[chunk], partner).wait_recv()
+        remote(at(rows), at(rows), ssem.at[0], rsem.at[chunk], partner).wait_recv()
 
     own_at = lambda r: zst.at[r]
     send_at = lambda r: send.at[r]
@@ -552,6 +550,9 @@
         halo_all().wait_recv()
 
     def finish():
+        most = pl.ds(0, ROWS - SLOT)
+        ends.append(remote(send.at[most], send.at[most], zi_send.at[0], zi_recv.at[0], partner))
+        ends.append(remote(res.at[most], res.at[most], zo_send.at[0], zo_recv.at[0], partner))
         out_ref[...] = sh_acc[...].astype(BF)
         for cp in ends:
             cp.wait_send()
@@ -646,8 +647,8 @@
     made = pl.pallas_call(
         kernel,
         out_shape=(
-            jax.ShapeDtypeStruct((LEN, 2 * HEAD_DIM), BF),
-            jax.ShapeDtypeStruct((TOK, FEAT), BF),
+            pltpu.VMEM((LEN, 2 * HEAD_DIM), BF),
+            pltpu.VMEM((TOK, FEAT), BF),
         ),
         in_specs=[hb] * 18,
         out_specs=(vm, vm),
@@ -687,16 +688,16 @@
             pltpu.VMEM((120, 128), BF),
             pltpu.VMEM((128, 120), BF),
             dma((2 * NGATHER,)),
-            dma((8 * NGATHER,)),
+            dma((6 * NGATHER,)),
+            dma((1,)),
             dma((NCHUNK,)),
-            dma((NCHUNK,)),
-            dma((NCHUNK,)),
+            dma((1,)),
             dma((NCHUNK,)),
             dma((2,)),
             dma((22,)),
         ],
         compiler_params=pltpu.CompilerParams(
-            collective_id=0, has_side_effects=True, vmem_limit_bytes=67043328
+            collective_id=0, has_side_effects=True, vmem_limit_bytes=66600000
         ),
         name="fused",
     )(
@@ -725,6 +726,7 @@
         in_specs=[vm, vm],
         out_specs=(hb, hb),
         scratch_shapes=[dma((2,))],
+        compiler_params=pltpu.CompilerParams(vmem_limit_bytes=2 * 1024 * 1024),
         name="deliver",
     )(*made)
 

time: 115 us -> 114 us (level); the launches traced: 115 us -> 113 us
  Pallas kernels: 114 us -> 112 us
    pallas_call x1, Pallas kernels: 113 us -> 111 us  [shards(): pl.pallas_call(kernel, out_shape=(pltpu.VMEM((LEN, 2 * HEAD_DIM), BF), pl...]
where the time goes in v1:
time: 114 us; the launch traced here: 113 us
  Pallas kernels  112 us (98%)
    pallas_call x1, Pallas kernels, shards(): pl.pallas_call(kernel, out_shape=(pltpu.VMEM((LEN, 2 * HEAD_DIM), BF), pl...  111 us

profile of v1, /device:TPU:1, one launch (start us, length us, event | category | flops | bytes accessed | tf_op | source)
XLA Modules:
  0.0 112.7 jit_solution(5448512327300493643)
XLA Ops:
  0.6 111.2 %fused.1 = (bf16[512,256]{1,0:T(8,128)(2,1)S(1)}, bf16[160,256]{1,0:T(8,128)(2,1)S(1)}) custom-call(bf16[160,256]{1,0:T(8,128)(2,1)} %x_hbm.1, s32[4,160]{1,0:T(4,128)} %bitcast.12, f32[4,160]{1,0:T(4,128)} %bitcast.13, bf16[512,256]{1,0:T(8,128)(2,1)} %q_hbm.1, bf16[512,128]{1,0:T(8,128)(2,1)} %k_hbm.1, bf16[512,128]{1,0:T(8,128)(2,1)} %v_hbm.1, ...), custom_call_target="tpu_custom_call" | custom-call | tf_op jit(solution)/shard_map/fused/pallas_call | solution.py:647
  111.8 0.7 deliver.1

commit v2 on v1

--- a/solution.py
+++ b/solution.py
@@ -28,7 +28,7 @@
 UNITS = 128
 PACK = 40
 
-GROUPS = [[1, -1], [5, -5], [6, -6], [8], [7, -7], [4, -4], [0], [3, -3], [2, -2]]
+GROUPS = [[3, -3], [8], [5, -5], [6, -6], [7, -7], [0], [4, -4], [2, -2], [1, -1]]
 REL = sum(GROUPS, [])
 NCHUNK = len(GROUPS)
 ZFIRST = [2 * SLOT * sum(len(g) for g in GROUPS[:c]) for c in range(NCHUNK)]
@@ -53,20 +53,20 @@
 
 ORDER = (
     "R9", "zi:0", "halo", "zi:1", "zi:2", "zi:3", "zi:4", "zi:5", "zi:6", "zi:7", "zi:8",
-    "cw", "lda", "lds", "ldb", "wi:6", "R6", "wi:0", "R0", "tq", "R9", "R6", "wh", "tk",
-    "R0", "at:0", "R9", "wi:1", "R1", "R0", "R6", "at:1", "R9", "R1", "R0", "wi:2", "R2",
-    "R9", "si", "H9", "R1", "R6", "wi:3", "R3", "R2", "R0", "ei:0", "H0", "R1", "R3", "R2",
-    "wi:4", "R4", "H9", "H0", "R6", "ei:6", "H6", "R1", "ei:1", "H1", "R2", "R3", "R4",
-    "wi:5", "R5", "H9", "H0", "H1", "wi:7", "R7", "R2", "ei:2", "H2", "R3", "R4", "R5",
-    "H9", "H0", "H1", "R7", "H2", "R3", "ei:3", "H3", "R4", "R5", "wi:8", "R8", "H9", "so",
-    "H1", "H0", "eo:0", "zo:0", "R7", "H2", "H3", "at:2", "R4", "ei:4", "H4", "R5", "H1",
-    "eo:1", "zo:1", "H3", "R7", "H2", "R8", "H4", "at:3", "R5", "ei:5", "H5", "H3", "R7",
-    "ei:7", "H7", "H2", "eo:2", "zo:2", "R8", "H4", "H5", "H3", "eo:3", "zo:3", "R8", "H4",
-    "H5", "H6", "H7", "wo:0", "cb:0-128", "wo:1", "cb:128-256", "R8", "ei:8", "H8", "H4",
-    "eo:4", "zo:4", "H5", "H6", "H7", "wo:2", "cb:256-384", "H8", "H5", "eo:5", "zo:5",
-    "H6", "H8", "H7", "H6", "eo:6", "zo:6", "H8", "H7", "eo:7", "zo:7", "H8", "eo:8",
-    "zo:8", "wo:3", "wo:4", "cb:384-512", "wo:5", "cb:512-640", "wo:6", "cb:640-768",
-    "wo:7", "cb:768-896", "wo:8", "cb:896-1024", "end",
+    "go", "cw", "lda", "tq", "wi:5", "R5", "R9", "wh", "tk", "at:0", "R5", "wi:0", "R0",
+    "at:1", "at:2", "at:3", "R9", "R0", "R5", "R9", "R0", "wi:1", "R1", "R5", "wi:2", "R2",
+    "R9", "lds", "si", "H9", "R0", "R1", "R5", "ldb", "ei:5", "H5", "R2", "H9", "wi:3",
+    "R3", "R0", "ei:0", "H0", "H5", "R2", "R1", "H9", "R3", "H0", "wi:4", "R4", "H5", "R2",
+    "H9", "R3", "R1", "H0", "R4", "H5", "R2", "ei:2", "H2", "H9", "so", "R4", "H0", "R3",
+    "wi:6", "R6", "R1", "ei:1", "H1", "H5", "eo:5", "zo:5", "H2", "wi:7", "R7", "R4", "H0",
+    "eo:0", "zo:0", "wi:8", "R8", "R3", "ei:3", "H3", "H1", "H2", "R6", "R7", "R4", "ei:4",
+    "H4", "H3", "H1", "R8", "wo:0", "cb:0-128", "H2", "R6", "R7", "H4", "H3", "H1", "R8",
+    "H2", "eo:2", "zo:2", "R6", "R7", "H4", "H3", "H1", "eo:1", "zo:1", "R8", "R6", "ei:6",
+    "H6", "H4", "R7", "ei:7", "H7", "H3", "eo:3", "zo:3", "H6", "R8", "ei:8", "H8", "H7",
+    "H4", "eo:4", "zo:4", "H6", "H8", "H7", "H6", "H8", "wo:1", "wo:2", "cb:128-256", "H7",
+    "H6", "eo:6", "zo:6", "H8", "H7", "eo:7", "zo:7", "wo:3", "cb:256-384", "H8", "eo:8",
+    "zo:8", "wo:4", "cb:384-512", "wo:5", "cb:512-640", "wo:6", "cb:640-768", "wo:7",
+    "cb:768-896", "wo:8", "cb:896-1024", "end",
 )
 
 
@@ -155,12 +155,10 @@
     ep_lo = (ep + 31) % 32
 
     barrier = pltpu.get_barrier_semaphore()
-    for p in range(NZ):
+    for rel in sorted(REL, key=abs, reverse=True)[:-1]:
         for c in range(2):
-            if REL[p] == 0:
-                continue
             pl.semaphore_signal(
-                barrier, inc=1, device_id={"ep": ep_at(REL[p], c), "tp": tp}, device_id_type=MESH
+                barrier, inc=1, device_id={"ep": ep_at(rel, c), "tp": tp}, device_id_type=MESH
             )
     pl.semaphore_signal(
         barrier, inc=1, device_id={"ep": z * 2 + (1 - core), "tp": tp}, device_id_type=MESH
@@ -183,26 +181,30 @@
         load(3, x_hbm, xpad.at[pl.ds(0, TOK)]),
     ]
     ld_kv = [load(4, k_hbm, kpad.at[mid]), load(5, v_hbm, vpad.at[mid])]
-    ld_att = [
-        load(6, q_hbm, q_ref),
-        load(7, qg_hbm, qg_ref),
-        load(8, kg_hbm, kg_ref),
-        load(9, sink_hbm, sink_ref),
-        load(10, colt_hbm, colt_ref),
-        load(11, rowt_hbm.at[:, pl.ds(pl.multiple_of(ep * 8, 8), 16), :], rowt),
-    ]
-    ld_shared = [load(12, sg_hbm, sg_ref), load(13, su_hbm, su_ref), load(14, ng_hbm, ng_ref)] + [
-        load(15 + j, sd_hbm, wsd.at[:, pl.ds(32 * j, 32), :]) for j in range(4)
-    ]
-    ld_big = [
-        load(19, gate_hbm.at[0], wgu.at[:, 0:128]),
-        load(20, up_hbm.at[0], wgu.at[:, 128:256]),
-        load(21, down_hbm.at[0], wd),
-    ]
-
     def wait_all(copies):
         for cp in copies:
             cp.wait()
+
+    late = {}
+
+    def start_loads():
+        ld_att = [
+            load(6, q_hbm, q_ref),
+            load(7, qg_hbm, qg_ref),
+            load(8, kg_hbm, kg_ref),
+            load(9, sink_hbm, sink_ref),
+            load(10, colt_hbm, colt_ref),
+            load(11, rowt_hbm.at[:, pl.ds(pl.multiple_of(ep * 8, 8), 16), :], rowt),
+        ]
+        ld_shared = [load(12, sg_hbm, sg_ref), load(13, su_hbm, su_ref), load(14, ng_hbm, ng_ref)] + [
+            load(15 + j, sd_hbm, wsd.at[:, pl.ds(32 * j, 32), :]) for j in range(4)
+        ]
+        ld_big = [
+            load(19, gate_hbm.at[0], wgu.at[:, 0:128]),
+            load(20, up_hbm.at[0], wgu.at[:, 128:256]),
+            load(21, down_hbm.at[0], wd),
+        ]
+        late.update(att=ld_att, shared=ld_shared, big=ld_big)
 
     xpad[TOK:TPAD, :] = jnp.zeros((TPAD - TOK, FEAT), BF)
     idsp[...] = jnp.full(idsp.shape, -1, jnp.int32)
@@ -250,7 +252,7 @@
         return r + over[0] + over[1] + over[2]
 
     iota = lambda shape, axis: lax.broadcasted_iota(jnp.int32, shape, axis)
-    wide_shape, tall_shape = (120, 128), (128, 120)
+    wide_shape, tall_shape = (128, 128), (128, 128)
     pick[...] = jnp.where(
         moved(iota(wide_shape, 0)) == iota(wide_shape, 1), 1.0, 0.0
     ).astype(BF)
@@ -472,7 +474,7 @@
             lhs[s, 0:size, :] = (f * ng_ref[:, pl.ds(pl.multiple_of(s * FEAT, FEAT), FEAT)]).astype(BF)
             return carry
 
-        lax.fori_loop(0, 16, one, 0)
+        lax.fori_loop(0, 16, one, 0, unroll=4)
         return lax.rsqrt(jnp.sum(acc[0:size, 0:128], axis=-1, keepdims=True) / D + EPS)
 
     def activate(g, u, factor):
@@ -573,9 +575,10 @@
         ei=experts_in,
         eo=experts_out,
         cb=combine,
-        lda=lambda: wait_all(ld_att),
-        lds=lambda: wait_all(ld_shared),
-        ldb=lambda: wait_all(ld_big),
+        go=start_loads,
+        lda=lambda: wait_all(late["att"]),
+        lds=lambda: wait_all(late["shared"]),
+        ldb=lambda: wait_all(late["big"]),
         end=finish,
     )
     for item in ORDER:
@@ -663,8 +666,8 @@
             pltpu.VMEM((2, GRID_W, HEAD_DIM), F32),
             pltpu.VMEM((32, D), BF),
             pltpu.VMEM((32, D), BF),
-            pltpu.VMEM((4, 4, PACKED + TOK, FEAT), BF),
-            pltpu.VMEM((4, 4, PACKED + PACK, UNITS), BF),
+            pltpu.VMEM((4, 4, PACKED + TOK + 24, FEAT), BF),
+            pltpu.VMEM((4, 4, PACKED + PACK + 16, UNITS), BF),
             pltpu.VMEM((D, 2 * UNITS), BF),
             pltpu.VMEM((16 * UNITS, FEAT), BF),
             pltpu.VMEM((16, 128, FEAT), BF),
@@ -685,8 +688,8 @@
             pltpu.VMEM((CHUNK, 128), F32),
             pltpu.VMEM((TOK, FEAT), F32),
             pltpu.VMEM((ROWS, FEAT), BF),
-            pltpu.VMEM((120, 128), BF),
-            pltpu.VMEM((128, 120), BF),
+            pltpu.VMEM((128, 128), BF),
+            pltpu.VMEM((128, 128), BF),
             dma((2 * NGATHER,)),
             dma((6 * NGATHER,)),
             dma((1,)),

time: 114 us -> 112 us (0.982)
  Pallas kernels: 112 us -> 109 us
    pallas_call x1, Pallas kernels: 111 us -> 109 us  [shards(): pl.pallas_call(kernel, out_shape=(pltpu.VMEM((LEN, 2 * HEAD_DIM), BF), pl...]
where the time goes in v2:
time: 112 us; the launch traced here: 110 us
  Pallas kernels  109 us (97%)
    pallas_call x1, Pallas kernels, shards(): pl.pallas_call(kernel, out_shape=(pltpu.VMEM((LEN, 2 * HEAD_DIM), BF), pl...  109 us

profile of v2, /device:TPU:1, one launch (start us, length us, event | category | flops | bytes accessed | tf_op | source)
XLA Modules:
  0.0 110.3 jit_solution(1880248142671597521)
XLA Ops:
  0.6 108.7 %fused.1 = (bf16[512,256]{1,0:T(8,128)(2,1)S(1)}, bf16[160,256]{1,0:T(8,128)(2,1)S(1)}) custom-call(bf16[160,256]{1,0:T(8,128)(2,1)} %x_hbm.1, s32[4,160]{1,0:T(4,128)} %bitcast.12, f32[4,160]{1,0:T(4,128)} %bitcast.13, bf16[512,256]{1,0:T(8,128)(2,1)} %q_hbm.1, bf16[512,128]{1,0:T(8,128)(2,1)} %k_hbm.1, bf16[512,128]{1,0:T(8,128)(2,1)} %v_hbm.1, ...), custom_call_target="tpu_custom_call" | custom-call | tf_op jit(solution)/shard_map/fused/pallas_call | solution.py:650
  109.4 0.7 deliver.1
